TPU v7x, 32 devices: a whole 2x2x4 slice. The times are simulated.
32 devices in a mesh: kv: 4 (over y, x), tp: 8 (over z, core).
Axes of the slice: x: 2, y: 2, z: 4, core: 2. Of those that a mesh axis runs over, the one named last changes fastest.
Arguments:
- tokens: bfloat16 [32, 4096], P(None, ('kv', 'tp')), may hold values from -60 to 60, as said below
- gain_mix: float32 [4096], replicated, may hold values from 0.1 to 1.9
- w_query: bfloat16 [4096, 4096], P('kv', 'tp'), may hold values from -0.09375 to 0.09375
- w_key: bfloat16 [4096, 4096], P('kv', 'tp'), may hold values from -0.75 to 0.75
- w_value: bfloat16 [4096, 4096], P('kv', 'tp'), may hold values from -0.09375 to 0.09375
- w_outgate: bfloat16 [4096, 4096], P('kv', 'tp'), may hold values from -0.09375 to 0.09375
- w_gates: bfloat16 [4096, 32], P('kv'), may hold values from -0.09375 to 0.09375
- forget_bias: float32 [16], replicated, may hold values from 0 to 4
- cell_state: float32 [32, 4096, 256], P('kv', 'tp'), may hold values from -1.5 to 1.5
- norm_state: float32 [32, 16, 256], P('kv'), may hold values from -1.5 to 1.5
- max_state: float32 [32, 16], P('kv'), may hold values from -1 to 2
- gain_group: float32 [4096], replicated, may hold values from 0.1 to 1.9
- w_mix: bfloat16 [4096, 4096], P('tp', 'kv'), may hold values from -0.125 to 0.125
- gain_ffn: float32 [4096], replicated, may hold values from 0.1 to 1.9
- w_up: bfloat16 [4096, 16384], P('kv', 'tp'), may hold values from -0.09375 to 0.09375
- w_down: bfloat16 [16384, 4096], P('tp', 'kv'), may hold values from -0.0625 to 0.0625
Outputs:
- layer_out: bfloat16 [32, 4096], P(None, ('kv', 'tp'))
- cell_next: float32 [32, 4096, 256], P('kv', 'tp')
- norm_next: float32 [32, 16, 256], P('kv')
- max_next: float32 [32, 16], P('kv')
Inputs may be any that keep to these rules, and one draw needn't show every extreme that they name: `tokens`: finite activations.
All inputs are finite; a program needn't handle non-finite values.
Results may differ from a plain program's by a relative error of at most 0.019.
Values may be sent and summed in bfloat16 or wider, within the bound.
A program may use at most 64 MiB of HBM per device.

v0:
```python
import math
import jax
import jax.numpy as jnp
from jax import lax
from jax.sharding import PartitionSpec as P

EPSILON = 1e-06


def per_device(
    tokens,
    gain_mix,
    w_query,
    w_key,
    w_value,
    w_outgate,
    w_gates,
    forget_bias,
    cell_state,
    norm_state,
    max_state,
    gain_group,
    w_mix,
    gain_ffn,
    w_up,
    w_down,
):
    f32 = jnp.float32
    bf16 = jnp.bfloat16
    exact = lax.Precision.HIGHEST
    width = gain_mix.shape[0]
    kv_index = lax.axis_index("kv")
    tp_index = lax.axis_index("tp")
    tokf = tokens.astype(f32)
    block_rows = lax.all_gather(tokens, "tp", axis=1, tiled=True)
    block = block_rows.shape[1]
    blockf = block_rows.astype(f32)
    gain_block = lax.dynamic_slice_in_dim(gain_mix, kv_index * block, block)
    normed = (blockf * gain_block).astype(bf16)
    partials = tuple(
        (
            jnp.dot(normed, weight, preferred_element_type=f32)
            for weight in (w_query, w_key, w_value, w_outgate, w_gates)
        )
    )
    partials = partials + (jnp.sum(blockf * blockf, axis=1),)
    summed = lax.psum_scatter(partials, "kv", scatter_dimension=0, tiled=True)
    seqs = summed[0].shape[0]
    seq_squares = summed[5]
    scale_in = lax.rsqrt(seq_squares / width + EPSILON)[:, None]
    query_part = (summed[0] * scale_in).astype(bf16)
    key_part = (summed[1] * scale_in).astype(bf16)
    values = summed[2] * scale_in
    gate_out = summed[3] * scale_in
    gates = summed[4] * scale_in
    query_all, key_all = (
        lax.all_gather(query_part, "tp", axis=1, tiled=True),
        lax.all_gather(key_part, "tp", axis=1, tiled=True),
    )
    heads = forget_bias.shape[0]
    head_dim = cell_state.shape[2]
    value_rows = cell_state.shape[1]
    queryf = query_all.astype(f32).reshape(seqs, heads, head_dim)
    keyf = key_all.astype(f32).reshape(seqs, heads, head_dim) / math.sqrt(head_dim)
    gate_in = gates[:, :heads]
    log_forget = jax.nn.log_sigmoid(gates[:, heads:] + forget_bias)
    max_next = jnp.maximum(log_forget + max_state, gate_in)
    decay = jnp.exp(log_forget + max_state - max_next)
    inflow = jnp.exp(gate_in - max_next)
    norm_next = decay[..., None] * norm_state + inflow[..., None] * keyf
    denom_heads = jnp.maximum(jnp.abs(jnp.sum(norm_next * queryf, axis=2)), 1.0)
    row_ids = tp_index * value_rows + jnp.arange(value_rows)
    select = (row_ids[:, None] // head_dim == jnp.arange(heads)[None, :]).astype(f32)
    query_rows = jnp.einsum("shd,rh->srd", queryf, select, precision=exact)
    key_rows = jnp.einsum("shd,rh->srd", keyf, select, precision=exact)
    decay_rows = jnp.einsum("sh,rh->sr", decay, select, precision=exact)
    inflow_rows = jnp.einsum("sh,rh->sr", inflow, select, precision=exact)
    denom_rows = jnp.einsum("sh,rh->sr", denom_heads, select, precision=exact)
    cell_next = (
        decay_rows[:, :, None] * cell_state
        + inflow_rows[:, :, None] * values[:, :, None] * key_rows
    )
    numer = jnp.sum(cell_next * query_rows, axis=2)
    cell_read = (jax.nn.sigmoid(gate_out) * (numer / denom_rows)).astype(bf16)
    read_rows = lax.all_gather(cell_read, "kv", axis=0, tiled=True)
    readf = read_rows.astype(f32)
    group_total = lax.psum(jnp.sum(readf * readf, axis=1), "tp")
    scale_group = lax.rsqrt(group_total / (heads * head_dim) + EPSILON)[:, None]
    gain_rows = lax.dynamic_slice_in_dim(gain_group, tp_index * value_rows, value_rows)
    grouped = (readf * gain_rows).astype(bf16)
    mix_terms = jnp.dot(grouped, w_mix, preferred_element_type=f32)
    mix_summed = lax.psum_scatter(mix_terms, "tp", scatter_dimension=1, tiled=True)
    mixed = (tokf + mix_summed * scale_group).astype(bf16)
    ffn_block = w_up.shape[0]
    piece = lax.all_gather(mixed, "tp", axis=1, tiled=True)
    count = piece.shape[1]
    piecef = piece.astype(f32)
    gain_piece = lax.dynamic_slice_in_dim(gain_ffn, kv_index * ffn_block, count)
    normed_piece = (piecef * gain_piece).astype(bf16)
    up_part = jnp.dot(normed_piece, w_up, preferred_element_type=f32)
    square_part = jnp.sum(piecef * piecef, axis=1)
    up_total, square_total = lax.psum((up_part, square_part), "kv")
    scale_ffn = lax.rsqrt(square_total / width + EPSILON)[:, None]
    hidden = jnp.square(jax.nn.relu(up_total * scale_ffn)).astype(bf16)
    down_terms = jnp.dot(hidden, w_down, preferred_element_type=f32)
    ffn_summed = lax.psum_scatter(down_terms, "tp", scatter_dimension=1, tiled=True)
    layer_out = (mixed.astype(f32) + ffn_summed).astype(bf16)
    return (layer_out, cell_next, norm_next, max_next)


def solution(mesh):
    in_specs = (
        P(None, ("kv", "tp")),
        P(),
        P("kv", "tp"),
        P("kv", "tp"),
        P("kv", "tp"),
        P("kv", "tp"),
        P("kv", None),
        P(),
        P("kv", "tp", None),
        P("kv", None, None),
        P("kv", None),
        P(),
        P("tp", "kv"),
        P(),
        P("kv", "tp"),
        P("tp", "kv"),
    )
    out_specs = (P(None, ("kv", "tp")), P("kv", "tp", None), P("kv", None, None), P("kv", None))
    return jax.shard_map(
        per_device, mesh=mesh, in_specs=in_specs, out_specs=out_specs, check_vma=False
    )
```

profile of v0, /device:TPU:0, one launch (start us, length us, event | category | flops | bytes accessed | tf_op | source)
XLA Modules:
  0.0 254.1 jit_solution(9708847309321128957)
XLA Ops:
  7.3 14.7 %all_gather.15 = bf16[32,1024]{1,0:T(8,128)(2,1)S(1)} all-gather(bf16[32,128]{1,0:T(8,128)(2,1)} %param.16), channel_id=1, replica_groups=mesh['kv'=4,'tp'=8] {'tp'}, dimensions={1}, use_global_device_ids=true | all-gather | bytes 73728 | tf_op jit(solution)/shard_map/all_gather | solution.py:35
  22.0 0.7 dynamic_slice.9
  22.7 2.1 fusion.31
  24.9 2.1 fusion.29
  27.0 2.1 fusion.27
  29.1 2.1 fusion.35
  32.9 16.5 %all-reduce.6 = (f32[32]{0:T(128)S(1)}, f32[32,32]{1,0:T(8,128)S(1)}) all-reduce(f32[32]{0:T(128)S(1)} %fusion.5, f32[32,32]{1,0:T(8,128)S(1)} %fusion.33), channel_id=3, replica_groups=mesh['kv'=4,'tp'=8] {'kv'}, use_global_device_ids=true, to_apply=%region_2.0.clone | all-reduce | flops 1056 | bytes 8448
  49.7 5.4 %copy.26 = f32[8,512,256]{1,2,0:T(8,128)} copy(f32[8,512,256]{2,1,0:T(8,128)} %param.24) | data formatting | bytes 8388608 | tf_op args[8]
  55.1 0.8 dynamic_slice.10
  56.0 18.8 %all-reduce.13.cloned.1.call-done = (f32[32,512]{1,0:T(8,128)}, f32[32,512]{1,0:T(8,128)}, f32[32,512]{1,0:T(8,128)}, f32[32,512]{1,0:T(8,128)}) async-done(((f32[32,512]{1,0:T(8,128)}, f32[32,512]{1,0:T(8,128)}, f32[32,512]{1,0:T(8,128)}, f32[32,512]{1,0:T(8,128)}), (f32[32,512]{1,0:T(8,128)}, f32[32,512]{1,0:T(8,128)}, f32[32,512]{1,0:T(8,128)}, f32[32,512]{1,0:T(8,128)})) %all-reduce.13.cloned.1.call-update) | async-done | bytes 262160
  74.8 0.9 convolution_multiply_fusion
  75.6 0.8 fusion.37
  76.4 14.0 %all_gather.16 = bf16[8,4096]{1,0:T(8,128)(2,1)S(1)} all-gather(bf16[8,512]{1,0:T(8,128)(2,1)S(1)} %get-tuple-element.23), channel_id=1, replica_groups=mesh['kv'=4,'tp'=8] {'tp'}, dimensions={1}, use_global_device_ids=true | all-gather | bytes 73728 | tf_op jit(solution)/shard_map/all_gather | solution.py:58
  90.4 14.0 %all_gather.17 = bf16[8,4096]{1,0:T(8,128)(2,1)S(1)} all-gather(bf16[8,512]{1,0:T(8,128)(2,1)S(1)} %get-tuple-element.22), channel_id=1, replica_groups=mesh['kv'=4,'tp'=8] {'tp'}, dimensions={1}, use_global_device_ids=true | all-gather | bytes 73728 | tf_op jit(solution)/shard_map/all_gather | solution.py:57
  104.4 4.3 %fusion.1 = f32[8,512,256]{1,2,0:T(8,128)S(1)} fusion(f32[8,512,256]{1,2,0:T(8,128)} %copy.26, f32[8,512]{1,0:T(8,128)S(1)} %convolution_multiply_fusion, f32[8,512]{1,0:T(8,128)S(1)} %fusion.24, f32[8,16,256]{2,0,1:T(8,128)S(1)} %convert.2, s32[512]{0:T(512)S(1)} %add_select_fusion), kind=kOutput, calls=%fused_computation.3 | convolution fusion | flops 204513280 | bytes 8554496 | tf_op jit(solution)/shard_map/shd,rh->srd/dot_general | solution.py:75
  108.7 1.9 copy-done.1
  110.6 0.8 fusion
  111.4 0.8 multiply_reduce_fusion
  112.2 0.9 fusion.3
  113.0 8.1 %all_gather.18 = bf16[32,512]{1,0:T(8,128)(2,1)S(1)} all-gather(bf16[8,512]{1,0:T(8,128)(2,1)S(1)} %fusion.3), channel_id=1, replica_groups=mesh['kv'=4,'tp'=8] {'kv'}, dimensions={0}, use_global_device_ids=true | all-gather | bytes 40960 | tf_op jit(solution)/shard_map/all_gather | solution.py:85
  121.2 0.9 fusion.20
  122.3 14.8 %psum.21 = f32[32]{0:T(128)S(1)} all-reduce(f32[32]{0:T(128)S(1)} %fusion.14), channel_id=1, replica_groups=mesh['kv'=4,'tp'=8] {'tp'}, use_global_device_ids=true, to_apply=%region_11.12 | all-reduce | flops 32 | bytes 256 | tf_op jit(solution)/shard_map/psum | solution.py:87
  137.2 15.7 %reduce-scatter.3.cloned.1.call-done = f32[32,128]{1,0:T(8,128)} async-done(((f32[32,1024]{1,0:T(8,128)}), f32[32,128]{1,0:T(8,128)}) %reduce-scatter.3.cloned.1.call-update) | async-done | bytes 16400 | tf_op jit(solution)/shard_map/reduce_scatter | solution.py:92
  152.9 0.8 add_convert_fusion.1
  153.7 12.7 %all_gather.19 = bf16[32,1024]{1,0:T(8,128)(2,1)S(1)} all-gather(bf16[32,128]{1,0:T(8,128)(2,1)S(1)} %add_convert_fusion.1), channel_id=1, replica_groups=mesh['kv'=4,'tp'=8] {'tp'}, dimensions={1}, use_global_device_ids=true | all-gather | bytes 73728 | tf_op jit(solution)/shard_map/all_gather | solution.py:95
  166.3 3.7 %fusion.15 = f32[32,2048]{1,0:T(8,128)} fusion(bf16[1024,2048]{1,0:T(8,128)(2,1)} %param.30, bf16[32,1024]{1,0:T(8,128)(2,1)S(1)} %all_gather.19, f32[1024]{0:T(1024)S(1)} %dynamic-slice-done), kind=kOutput, calls=%fused_computation.28 | convolution fusion | flops 134316032 | bytes 4526080 | tf_op jit(solution)/shard_map/dot_general | solution.py:100
  170.3 10.0 %psum.23 = f32[32]{0:T(128)S(1)} all-reduce(f32[32]{0:T(128)S(1)} %fusion.7), channel_id=1, replica_groups=mesh['kv'=4,'tp'=8] {'kv'}, use_global_device_ids=true, to_apply=%region_14.15 | all-reduce | flops 32 | bytes 256 | tf_op jit(solution)/shard_map/psum | solution.py:102
  180.2 31.5 %all-reduce.11.cloned.1.call-done = f32[32,2048]{1,0:T(8,128)} async-done(((f32[32,2048]{1,0:T(8,128)}), f32[32,2048]{1,0:T(8,128)}) %all-reduce.11.cloned.1.call-update) | async-done | bytes 262160 | tf_op jit(solution)/shard_map/psum | solution.py:102
  211.7 3.8 %fusion.8 = f32[32,1024]{1,0:T(8,128)} fusion(bf16[2048,1024]{1,0:T(8,128)(2,1)} %param.31, f32[32,2048]{1,0:T(8,128)} %all-reduce.11.cloned.1.call-done, f32[32]{0:T(128)S(1)} %add_rsqrt_fusion), kind=kOutput, calls=%fused_computation.17 | convolution fusion | flops 134479872 | bytes 4587648 | tf_op jit(solution)/shard_map/dot_general | solution.py:105
  215.6 5.3 %copy.31 = f32[8,512,256]{2,1,0:T(8,128)} copy(f32[8,512,256]{1,2,0:T(8,128)} %copy-done.1) | data formatting | bytes 8388608
  220.9 25.3 %reduce-scatter.5.cloned.1.call-done = f32[32,128]{1,0:T(8,128)} async-done(((f32[32,1024]{1,0:T(8,128)}), f32[32,128]{1,0:T(8,128)}) %reduce-scatter.5.cloned.1.call-update) | async-done | bytes 16400 | tf_op jit(solution)/shard_map/reduce_scatter | solution.py:106
  246.2 1.3 add_convert_fusion
  (41 shorter events, 1.9 us)
Async XLA Ops:
  7.2 114.0 %copy-start = (bf16[512,1024]{1,0:T(8,128)(2,1)S(1)}, bf16[512,1024]{1,0:T(8,128)(2,1)}, u32[]{:S(2)}) copy-start(bf16[512,1024]{1,0:T(8,128)(2,1)} %param.28) | copy-start | bytes 3145732
  7.2 24.4 %copy-start.8 = (u32[32]{0:T(128)S(1)}, u32[32]{0:T(128)}, u32[]{:S(2)}) copy-start(u32[32]{0:T(128)} %constant.55) | copy-start | bytes 388
  7.2 24.3 %copy-start.3 = (bf16[1024,32]{0,1:T(8,128)(2,1)S(1)}, bf16[1024,32]{0,1:T(8,128)(2,1)}, u32[]{:S(2)}) copy-start(bf16[1024,32]{0,1:T(8,128)(2,1)} %param.22) | copy-start | bytes 196612
  7.2 42.3 %copy-start.5 = (f32[8,16]{1,0:T(8,128)S(1)}, f32[8,16]{1,0:T(8,128)}, u32[]{:S(2)}) copy-start(f32[8,16]{1,0:T(8,128)} %param.26) | copy-start | bytes 1540
  7.2 42.3 %copy-start.7 = (f32[16]{0:T(128)S(1)}, f32[16]{0:T(128)}, u32[]{:S(2)}) copy-start(f32[16]{0:T(128)} %param.23) | copy-start | bytes 196
  7.2 67.5 %all-reduce.13.cloned.1.call-start = ((), (), s32[]{:S(2)}) async-start(), calls=%async_computation.5 | async-start | bytes 524288
  31.3 121.6 %reduce-scatter.3.cloned.1.call-start = ((), (), s32[]{:S(2)}) async-start(), calls=%async_computation.2 | async-start | bytes 147456 | tf_op jit(solution)/shard_map/reduce_scatter | solution.py:92
  49.6 25.2 %copy-start.6 = (f32[8,16]{1,0:T(8,128)}, f32[8,16]{1,0:T(8,128)S(1)}, u32[]{:S(2)}) copy-start(f32[8,16]{1,0:T(8,128)S(1)} %get-tuple-element.21) | copy-start | bytes 1540
  108.7 1.9 copy-start.1
  108.7 2.7 %copy-start.2 = (f32[8,16,256]{2,1,0:T(8,128)S(1)}, f32[8,16,256]{2,1,0:T(8,128)}, u32[]{:S(2)}) copy-start(f32[8,16,256]{2,1,0:T(8,128)} %param.25) | copy-start | bytes 393220
  108.7 44.1 %copy-start.4 = (bf16[32,128]{1,0:T(8,128)(2,1)S(1)}, bf16[32,128]{1,0:T(8,128)(2,1)}, u32[]{:S(2)}) copy-start(bf16[32,128]{1,0:T(8,128)(2,1)} %param.16) | copy-start | bytes 24580
  108.7 57.6 %dynamic-slice-start = ((f32[4096]{0:T(1024)}, s32[]{:T(128)}), f32[1024]{0:T(1024)S(1)}, s32[]{:S(2)}) async-start(f32[4096]{0:T(1024)} %param.29, s32[]{:T(128)} %select_n.22), calls=%async_computation.6 | async-start | bytes 8704 | tf_op jit(solution)/shard_map/dynamic_slice | solution.py:98
  122.1 89.6 %all-reduce.11.cloned.1.call-start = ((), (), s32[]{:S(2)}) async-start(), calls=%async_computation.3 | async-start | bytes 524288 | tf_op jit(solution)/shard_map/psum | solution.py:102
  170.1 76.2 %reduce-scatter.5.cloned.1.call-start = ((), (), s32[]{:S(2)}) async-start(), calls=%async_computation.4 | async-start | bytes 147456 | tf_op jit(solution)/shard_map/reduce_scatter | solution.py:106
Sparse Core Ops, SparseCore 0:
  31.4 43.3 all-reduce.12
  122.3 30.5 reduce-scatter.2
  170.2 41.4 all-reduce.10
  215.7 30.5 reduce-scatter.4
where the time goes:
time: 255 us; the launch traced here: 254 us
  blocking collectives  105 us (41%)
  waiting for transfers between devices  91.4 us (36%)
  matrix products  24 us (9%)
  local copies, waits for them, and re-layouts  14.7 us (6%)
  between operations  14.6 us (6%)
  other arithmetic  4.42 us (2%)
    psum x1, waiting for transfers between devices, per_device(): up_total, square_total = lax.psum((up_part, square_part), 'kv')  31.5 us
    reduce_scatter x1, waiting for transfers between devices, per_device(): lax.psum_scatter(down_terms, 'tp', scatter_dimension=1, tiled=True)  25.3 us
    unnamed x5, waiting for transfers between devices  18.8 us
    unnamed x1, blocking collectives  16.5 us
    reduce_scatter x1, waiting for transfers between devices, per_device(): lax.psum_scatter(mix_terms, 'tp', scatter_dimension=1, tiled=True)  15.7 us
    psum x1, blocking collectives, per_device(): group_total = lax.psum(jnp.sum(readf * readf, axis=1), 'tp')  14.8 us
    all_gather x1, blocking collectives, per_device(): block_rows = lax.all_gather(tokens, 'tp', axis=1, tiled=True)  14.7 us
    all_gather x1, blocking collectives, per_device(): lax.all_gather(query_part, 'tp', axis=1, tiled=True)  14 us
  transfers between devices with their start and end apart: 4, of which 4 were waited for; matrix products, arithmetic and copies ran while one was open for 5% of the time, Pallas kernels for 0%

commit v1 on v0

--- a/solution.py
+++ b/solution.py
@@ -55,7 +55,9 @@
     gates = summed[4] * scale_in
     query_all, key_all = (
         lax.all_gather(query_part, "tp", axis=1, tiled=True),
-        lax.all_gather(key_part, "tp", axis=1, tiled=True),
+        jnp.concatenate(
+            lax.all_to_all(jnp.stack([key_part] * lax.axis_size("tp")), "tp", 0, 0), axis=1
+        ),
     )
     heads = forget_bias.shape[0]
     head_dim = cell_state.shape[2]

time: 255 us -> 247 us (0.969)
  blocking collectives: 105 us -> 91.4 us
  starting transfers between devices: 0.16 us -> 4.76 us
    all_gather x1 -> x0, blocking collectives: 14 us -> none  [per_device(): lax.all_gather(key_part, 'tp', axis=1, tiled=True)]
    all_to_all x0 -> x1, starting transfers between devices: none -> 4.61 us  [per_device(): lax.all_to_all(jnp.stack([key_part] * lax.axis_size('tp')), 'tp', 0, 0)]
  transfers between devices with their start and end apart: 4 -> 5, of which waited for: 4 -> 4; matrix products, arithmetic and copies ran while one was open for 5% -> 6% of each run, Pallas kernels for 0% -> 0%
where the time goes in v1:
time: 247 us; the launch traced here: 246 us
  blocking collectives  91.4 us (37%)
  waiting for transfers between devices  91.4 us (37%)
  matrix products  24 us (10%)
  local copies, waits for them, and re-layouts  15.4 us (6%)
  between operations  14.6 us (6%)
  starting transfers between devices  4.76 us (2%)
  other arithmetic  4.41 us (2%)
    psum x1, waiting for transfers between devices, per_device(): up_total, square_total = lax.psum((up_part, square_part), 'kv')  31.5 us
    reduce_scatter x1, waiting for transfers between devices, per_device(): lax.psum_scatter(down_terms, 'tp', scatter_dimension=1, tiled=True)  25.3 us
    unnamed x5, waiting for transfers between devices  18.8 us
    unnamed x1, blocking collectives  16.6 us
    reduce_scatter x1, waiting for transfers between devices, per_device(): lax.psum_scatter(mix_terms, 'tp', scatter_dimension=1, tiled=True)  15.7 us
    psum x1, blocking collectives, per_device(): group_total = lax.psum(jnp.sum(readf * readf, axis=1), 'tp')  14.8 us
    all_gather x1, blocking collectives, per_device(): block_rows = lax.all_gather(tokens, 'tp', axis=1, tiled=True)  14.7 us
    all_gather x1, blocking collectives, per_device(): lax.all_gather(query_part, 'tp', axis=1, tiled=True)  14.5 us
  transfers between devices with their start and end apart: 5, of which 4 were waited for; matrix products, arithmetic and copies ran while one was open for 6% of the time, Pallas kernels for 0%

profile of v1, /device:TPU:0, one launch (start us, length us, event | category | flops | bytes accessed | tf_op | source)
XLA Modules:
  0.0 246.0 jit_solution(1035024286530786140)
XLA Ops:
  7.3 14.7 %all_gather.12 = bf16[32,1024]{1,0:T(8,128)(2,1)S(1)} all-gather(bf16[32,128]{1,0:T(8,128)(2,1)} %param.16), channel_id=1, replica_groups=mesh['kv'=4,'tp'=8] {'tp'}, dimensions={1}, use_global_device_ids=true | all-gather | bytes 73728 | tf_op jit(solution)/shard_map/all_gather | solution.py:35
  22.0 0.7 dynamic_slice.9
  22.7 2.1 fusion.30
  24.9 2.1 fusion.28
  27.0 2.1 fusion.26
  29.1 2.1 fusion.34
  32.8 16.6 %all-reduce.6 = (f32[32]{0:T(128)S(1)}, f32[32,32]{1,0:T(8,128)S(1)}) all-reduce(f32[32]{0:T(128)S(1)} %fusion.5, f32[32,32]{1,0:T(8,128)S(1)} %fusion.32), channel_id=3, replica_groups=mesh['kv'=4,'tp'=8] {'kv'}, use_global_device_ids=true, to_apply=%region_2.0.clone | all-reduce | flops 1056 | bytes 8448
  49.8 5.4 %copy.24 = f32[8,512,256]{1,2,0:T(8,128)} copy(f32[8,512,256]{2,1,0:T(8,128)} %param.24) | data formatting | bytes 8388608 | tf_op args[8]
  55.1 0.8 dynamic_slice.10
  56.0 18.8 %all-reduce.13.cloned.1.call-done = (f32[32,512]{1,0:T(8,128)}, f32[32,512]{1,0:T(8,128)}, f32[32,512]{1,0:T(8,128)}, f32[32,512]{1,0:T(8,128)}) async-done(((f32[32,512]{1,0:T(8,128)}, f32[32,512]{1,0:T(8,128)}, f32[32,512]{1,0:T(8,128)}, f32[32,512]{1,0:T(8,128)}), (f32[32,512]{1,0:T(8,128)}, f32[32,512]{1,0:T(8,128)}, f32[32,512]{1,0:T(8,128)}, f32[32,512]{1,0:T(8,128)})) %all-reduce.13.cloned.1.call-update) | async-done | bytes 262160
  74.8 0.8 fusion.36
  76.2 4.6 %all-to-all-start = ((bf16[8,8,512]{2,1,0:T(8,128)(2,1)}), bf16[8,8,512]{2,1,0:T(8,128)(2,1)S(1)}, u32[]{:S(2)}, u32[]{:S(2)}) async-start(bf16[8,8,512]{2,1,0:T(8,128)(2,1)} %stack.2), calls=%async_computation | async-start | bytes 131072 | tf_op jit(solution)/shard_map/all_to_all | solution.py:59
  80.9 0.9 convolution_multiply_fusion
  81.8 14.5 %all_gather.13 = bf16[8,4096]{1,0:T(8,128)(2,1)S(1)} all-gather(bf16[8,512]{1,0:T(8,128)(2,1)S(1)} %get-tuple-element.22), channel_id=1, replica_groups=mesh['kv'=4,'tp'=8] {'tp'}, dimensions={1}, use_global_device_ids=true | all-gather | bytes 73728 | tf_op jit(solution)/shard_map/all_gather | solution.py:57
  96.3 4.3 %fusion.1 = f32[8,512,256]{1,2,0:T(8,128)S(1)} fusion(f32[8,512,256]{1,2,0:T(8,128)} %copy.24, f32[8,512]{1,0:T(8,128)S(1)} %convolution_multiply_fusion, f32[8,512]{1,0:T(8,128)S(1)} %fusion.23, f32[8,16,256]{2,1,0:T(8,128)S(1)} %reshape.73, s32[512]{0:T(512)S(1)} %add_select_fusion), kind=kOutput, calls=%fused_computation.3 | convolution fusion | flops 204513280 | bytes 8554496 | tf_op jit(solution)/shard_map/shd,rh->srd/dot_general | solution.py:77
  100.7 1.9 copy-done.1
  102.6 0.8 fusion
  103.3 0.8 multiply_reduce_fusion
  104.1 0.9 fusion.3
  105.0 8.1 %all_gather.14 = bf16[32,512]{1,0:T(8,128)(2,1)S(1)} all-gather(bf16[8,512]{1,0:T(8,128)(2,1)S(1)} %fusion.3), channel_id=1, replica_groups=mesh['kv'=4,'tp'=8] {'kv'}, dimensions={0}, use_global_device_ids=true | all-gather | bytes 40960 | tf_op jit(solution)/shard_map/all_gather | solution.py:87
  113.1 0.9 fusion.19
  114.2 14.8 %psum.21 = f32[32]{0:T(128)S(1)} all-reduce(f32[32]{0:T(128)S(1)} %fusion.13), channel_id=1, replica_groups=mesh['kv'=4,'tp'=8] {'tp'}, use_global_device_ids=true, to_apply=%region_11.12 | all-reduce | flops 32 | bytes 256 | tf_op jit(solution)/shard_map/psum | solution.py:89
  129.1 15.7 %reduce-scatter.3.cloned.1.call-done = f32[32,128]{1,0:T(8,128)} async-done(((f32[32,1024]{1,0:T(8,128)}), f32[32,128]{1,0:T(8,128)}) %reduce-scatter.3.cloned.1.call-update) | async-done | bytes 16400 | tf_op jit(solution)/shard_map/reduce_scatter | solution.py:94
  144.8 0.8 add_convert_fusion.1
  145.6 12.7 %all_gather.15 = bf16[32,1024]{1,0:T(8,128)(2,1)S(1)} all-gather(bf16[32,128]{1,0:T(8,128)(2,1)S(1)} %add_convert_fusion.1), channel_id=1, replica_groups=mesh['kv'=4,'tp'=8] {'tp'}, dimensions={1}, use_global_device_ids=true | all-gather | bytes 73728 | tf_op jit(solution)/shard_map/all_gather | solution.py:97
  158.2 3.7 %fusion.14 = f32[32,2048]{1,0:T(8,128)} fusion(bf16[1024,2048]{1,0:T(8,128)(2,1)} %param.30, bf16[32,1024]{1,0:T(8,128)(2,1)S(1)} %all_gather.15, f32[1024]{0:T(1024)S(1)} %dynamic-slice-done), kind=kOutput, calls=%fused_computation.28 | convolution fusion | flops 134316032 | bytes 4526080 | tf_op jit(solution)/shard_map/dot_general | solution.py:102
  162.2 10.0 %psum.23 = f32[32]{0:T(128)S(1)} all-reduce(f32[32]{0:T(128)S(1)} %fusion.7), channel_id=1, replica_groups=mesh['kv'=4,'tp'=8] {'kv'}, use_global_device_ids=true, to_apply=%region_14.15 | all-reduce | flops 32 | bytes 256 | tf_op jit(solution)/shard_map/psum | solution.py:104
  172.1 31.5 %all-reduce.11.cloned.1.call-done = f32[32,2048]{1,0:T(8,128)} async-done(((f32[32,2048]{1,0:T(8,128)}), f32[32,2048]{1,0:T(8,128)}) %all-reduce.11.cloned.1.call-update) | async-done | bytes 262160 | tf_op jit(solution)/shard_map/psum | solution.py:104
  203.6 3.8 %fusion.8 = f32[32,1024]{1,0:T(8,128)} fusion(bf16[2048,1024]{1,0:T(8,128)(2,1)} %param.31, f32[32,2048]{1,0:T(8,128)} %all-reduce.11.cloned.1.call-done, f32[32]{0:T(128)S(1)} %add_rsqrt_fusion), kind=kOutput, calls=%fused_computation.17 | convolution fusion | flops 134479872 | bytes 4587648 | tf_op jit(solution)/shard_map/dot_general | solution.py:107
  207.5 5.3 %copy.28 = f32[8,512,256]{2,1,0:T(8,128)} copy(f32[8,512,256]{1,2,0:T(8,128)} %copy-done.1) | data formatting | bytes 8388608
  212.8 25.3 %reduce-scatter.5.cloned.1.call-done = f32[32,128]{1,0:T(8,128)} async-done(((f32[32,1024]{1,0:T(8,128)}), f32[32,128]{1,0:T(8,128)}) %reduce-scatter.5.cloned.1.call-update) | async-done | bytes 16400 | tf_op jit(solution)/shard_map/reduce_scatter | solution.py:108
  238.2 1.3 add_convert_fusion
  (45 shorter events, 2.6 us)
Async XLA Ops:
  7.2 105.9 %copy-start = (bf16[512,1024]{1,0:T(8,128)(2,1)S(1)}, bf16[512,1024]{1,0:T(8,128)(2,1)}, u32[]{:S(2)}) copy-start(bf16[512,1024]{1,0:T(8,128)(2,1)} %param.28) | copy-start | bytes 3145732
  7.2 24.4 %copy-start.8 = (u32[32]{0:T(128)S(1)}, u32[32]{0:T(128)}, u32[]{:S(2)}) copy-start(u32[32]{0:T(128)} %constant.55) | copy-start | bytes 388
  7.2 24.2 %copy-start.3 = (bf16[1024,32]{0,1:T(8,128)(2,1)S(1)}, bf16[1024,32]{0,1:T(8,128)(2,1)}, u32[]{:S(2)}) copy-start(bf16[1024,32]{0,1:T(8,128)(2,1)} %param.22) | copy-start | bytes 196612
  7.2 42.3 %copy-start.5 = (f32[8,16]{1,0:T(8,128)S(1)}, f32[8,16]{1,0:T(8,128)}, u32[]{:S(2)}) copy-start(f32[8,16]{1,0:T(8,128)} %param.26) | copy-start | bytes 1540
  7.2 42.3 %copy-start.7 = (f32[16]{0:T(128)S(1)}, f32[16]{0:T(128)}, u32[]{:S(2)}) copy-start(f32[16]{0:T(128)} %param.23) | copy-start | bytes 196
  7.2 67.6 %all-reduce.13.cloned.1.call-start = ((), (), s32[]{:S(2)}) async-start(), calls=%async_computation.6 | async-start | bytes 524288
  49.6 31.2 %copy-start.6 = (f32[8,16]{1,0:T(8,128)}, f32[8,16]{1,0:T(8,128)S(1)}, u32[]{:S(2)}) copy-start(f32[8,16]{1,0:T(8,128)S(1)} %get-tuple-element.21) | copy-start | bytes 1540
  76.2 20.0 %all-to-all-start = ((bf16[8,8,512]{2,1,0:T(8,128)(2,1)}), bf16[8,8,512]{2,1,0:T(8,128)(2,1)S(1)}, u32[]{:S(2)}, u32[]{:S(2)}) async-start(bf16[8,8,512]{2,1,0:T(8,128)(2,1)} %stack.2), calls=%async_computation | async-start | bytes 131072 | tf_op jit(solution)/shard_map/all_to_all | solution.py:59
  80.8 63.9 %reduce-scatter.3.cloned.1.call-start = ((), (), s32[]{:S(2)}) async-start(), calls=%async_computation.3 | async-start | bytes 147456 | tf_op jit(solution)/shard_map/reduce_scatter | solution.py:94
  100.6 1.9 copy-start.1
  100.6 2.7 %copy-start.2 = (f32[8,16,256]{2,1,0:T(8,128)S(1)}, f32[8,16,256]{2,1,0:T(8,128)}, u32[]{:S(2)}) copy-start(f32[8,16,256]{2,1,0:T(8,128)} %param.25) | copy-start | bytes 393220
  100.6 44.1 %copy-start.4 = (bf16[32,128]{1,0:T(8,128)(2,1)S(1)}, bf16[32,128]{1,0:T(8,128)(2,1)}, u32[]{:S(2)}) copy-start(bf16[32,128]{1,0:T(8,128)(2,1)} %param.16) | copy-start | bytes 24580
  100.7 57.6 %dynamic-slice-start = ((f32[4096]{0:T(1024)}, s32[]{:T(128)}), f32[1024]{0:T(1024)S(1)}, s32[]{:S(2)}) async-start(f32[4096]{0:T(1024)} %param.29, s32[]{:T(128)} %select_n.22), calls=%async_computation.7 | async-start | bytes 8704 | tf_op jit(solution)/shard_map/dynamic_slice | solution.py:100
  114.1 89.6 %all-reduce.11.cloned.1.call-start = ((), (), s32[]{:S(2)}) async-start(), calls=%async_computation.4 | async-start | bytes 524288 | tf_op jit(solution)/shard_map/psum | solution.py:104
  162.0 76.2 %reduce-scatter.5.cloned.1.call-start = ((), (), s32[]{:S(2)}) async-start(), calls=%async_computation.5 | async-start | bytes 147456 | tf_op jit(solution)/shard_map/reduce_scatter | solution.py:108
Sparse Core Ops, SparseCore 0:
  31.4 43.3 all-reduce.12
  114.2 30.5 reduce-scatter.2
  162.1 41.4 all-reduce.10
  207.6 30.5 reduce-scatter.4
